TPU v7x, 32 devices: a whole 2x2x4 slice. The times are simulated.
32 devices in a mesh: tp: 8 (over z, y), dp: 4 (over x, core).
Axes of the slice: x: 2, y: 2, z: 4, core: 2. Of those that a mesh axis runs over, the one named last changes fastest.
Arguments:
- stream: bfloat16 [128, 4096], P(None, ('dp', 'tp')), may hold values from -16 to 16
- lengths: int32 [128], P('dp'), may hold values from 1 to 64, 1024 in all
- prior_state: float32 [2, 128, 4096], P(None, 'dp', 'tp'), may hold values from -6 to 6
- prior_window: bfloat16 [2, 128, 3, 4096], P(None, 'dp', None, 'tp'), may hold values from -6 to 6
- norm_gain: float32 [2, 4096], P(None, 'dp'), may hold values from 0.1 to 1.9
- w_branch: bfloat16 [2, 4096, 4096], P(None, 'dp', 'tp'), may hold values from -0.09375 to 0.09375
- w_gate_branch: bfloat16 [2, 4096, 4096], P(None, 'dp', 'tp'), may hold values from -0.09375 to 0.09375
- conv_taps: bfloat16 [2, 4, 4096], P(None, None, 'tp'), may hold values from -3 to 3
- w_in_gate: bfloat16 [2, 256, 4096], P(None, None, 'tp'), may hold values from -0.375 to 0.375
- w_rec_gate: bfloat16 [2, 256, 4096], P(None, None, 'tp'), may hold values from -0.375 to 0.375
- decay_param: float32 [2, 4096], P(None, 'tp'), may hold values from -1 to 4
- w_out: bfloat16 [2, 4096, 4096], P(None, 'tp', 'dp'), may hold values from -0.1875 to 0.1875
Outputs:
- mixed_out: bfloat16 [128, 4096], P(None, ('dp', 'tp'))
- new_state: float32 [2, 128, 4096], P(None, 'dp', 'tp')
- new_window: bfloat16 [2, 128, 3, 4096], P(None, 'dp', None, 'tp')
All inputs are finite; a program needn't handle non-finite values. No bound on the sum of `lengths` on one device may be relied on, other than what follows from the above.
Results may differ from a plain program's by a relative error of at most 0.014.
Values may be sent and summed in bfloat16 or wider, within the bound.
A program may use at most 64 MiB of HBM per device.

v0:
```python
import jax
import jax.numpy as jnp
from jax import lax
from jax.sharding import PartitionSpec as P

D = 4096
BLOCK = 256
epsilon = 1e-06


def from_partner(block, axis, apart):
    count = lax.axis_size(axis)
    route = []
    for low in range(count):
        high = low | 1 << apart
        if high != low and high < count:
            route += [(low, high), (high, low)]
    return lax.ppermute(block, axis, route)


def norm_rows(block_rows, gain_values, squares):
    scaling = lax.rsqrt(squares / D + epsilon)
    return (block_rows.astype(jnp.float32) * scaling * gain_values).astype(jnp.bfloat16)


def normed_input(stream_local, gain_block):
    own_width = stream_local.shape[1]
    offset = lax.axis_index("tp") * own_width
    widened = stream_local.astype(jnp.float32)
    squares = lax.psum(jnp.sum(widened * widened, axis=1, keepdims=True), ("tp", "dp"))
    own_gain = lax.dynamic_slice_in_dim(gain_block, offset, own_width, 0)
    result = lax.all_gather(norm_rows(stream_local, own_gain, squares), "tp", axis=1, tiled=True)
    return result


def peer_block(convolved):
    col_count = convolved.shape[1]
    group_size = max(BLOCK // col_count, 1)
    device = lax.axis_index("tp")
    grouped = convolved
    for bit_number in range(group_size.bit_length() - 1):
        partner = from_partner(grouped, "tp", bit_number)
        is_upper = device // (1 << bit_number) % 2 == 1
        grouped = jnp.where(
            is_upper,
            jnp.concatenate([partner, grouped], axis=1),
            jnp.concatenate([grouped, partner], axis=1),
        )
    return grouped


def block_gates(grouped, weight):
    row_count = grouped.shape[0]
    col_count = weight.shape[1]
    blocks = max(col_count // BLOCK, 1)
    block_cols = min(col_count, BLOCK)
    inputs = grouped.reshape(row_count, blocks, BLOCK)
    tables = weight.reshape(BLOCK, blocks, block_cols)
    mapped = jnp.einsum("rnk,knc->rnc", inputs, tables, preferred_element_type=jnp.float32)
    return mapped.reshape(row_count, col_count)


def recurrent_step(
    normed,
    lengths,
    prior_state,
    prior_window,
    w_branch,
    w_gate_branch,
    conv_taps,
    w_in_gate,
    w_rec_gate,
    decay_param,
    w_out,
    stream_local,
):
    col_count = w_branch.shape[1]
    summed = lax.psum_scatter(
        jnp.concatenate(
            [
                jnp.dot(normed, w_branch, preferred_element_type=jnp.float32),
                jnp.dot(normed, w_gate_branch, preferred_element_type=jnp.float32),
            ],
            axis=1,
        ).astype(jnp.bfloat16),
        "dp",
        scatter_dimension=0,
        tiled=True,
    ).astype(jnp.float32)
    branch = summed[:, :col_count].astype(jnp.bfloat16)
    gate_in = summed[:, col_count:].astype(jnp.bfloat16)
    depth = prior_window.shape[1]
    needed = depth + 1 - jnp.arange(depth, dtype=jnp.int32)
    living = lengths[:, None, None] >= needed[None, :, None]
    history = jnp.where(living, prior_window, jnp.zeros_like(prior_window))
    window = jnp.concatenate([history, branch[:, None, :]], axis=1)
    convolved = jnp.sum(
        window.astype(jnp.float32) * conv_taps.astype(jnp.float32)[None], axis=1
    ).astype(jnp.bfloat16)
    grouped = peer_block(convolved)
    input_gate = jax.nn.sigmoid(block_gates(grouped, w_in_gate))
    recur_gate = jax.nn.sigmoid(block_gates(grouped, w_rec_gate))
    log_keep = 8.0 * recur_gate * jax.nn.log_sigmoid(decay_param)
    keeping = jnp.exp(log_keep)
    feeding = jnp.sqrt(-jnp.expm1(2.0 * log_keep))
    earlier = jnp.where(lengths[:, None] >= 2, prior_state, jnp.zeros_like(prior_state))
    state = keeping * earlier + feeding * input_gate * convolved.astype(jnp.float32)
    readout = (state * jax.nn.gelu(gate_in.astype(jnp.float32))).astype(jnp.bfloat16)
    mixed = jnp.dot(
        lax.all_gather(readout, "dp", axis=0, tiled=True), w_out, preferred_element_type=jnp.float32
    )
    own_width = stream_local.shape[1]
    offset = lax.axis_index("tp") * own_width
    own_cols = lax.dynamic_slice_in_dim(mixed, offset, own_width, 1) + stream_local.astype(
        jnp.float32
    )
    terms = lax.dynamic_update_slice_in_dim(mixed, own_cols, offset, 1)
    return (terms, state, window[:, 1:])


def body(
    stream,
    lengths,
    prior_state,
    prior_window,
    norm_gain,
    w_branch,
    w_gate_branch,
    conv_taps,
    w_in_gate,
    w_rec_gate,
    decay_param,
    w_out,
):
    normed = normed_input(stream, norm_gain[0])
    terms, state_first, window_first = recurrent_step(
        normed,
        lengths,
        prior_state[0],
        prior_window[0],
        w_branch[0],
        w_gate_branch[0],
        conv_taps[0],
        w_in_gate[0],
        w_rec_gate[0],
        decay_param[0],
        w_out[0],
        stream,
    )
    carried = lax.psum(terms, "tp").astype(jnp.bfloat16)
    widened = carried.astype(jnp.float32)
    squares = lax.psum(jnp.sum(widened * widened, axis=1, keepdims=True), "dp")
    normed = norm_rows(carried, norm_gain[1], squares)
    own_width = stream.shape[1]
    first = lax.dynamic_slice_in_dim(carried, lax.axis_index("tp") * own_width, own_width, 1)
    terms, state_second, window_second = recurrent_step(
        normed,
        lengths,
        prior_state[1],
        prior_window[1],
        w_branch[1],
        w_gate_branch[1],
        conv_taps[1],
        w_in_gate[1],
        w_rec_gate[1],
        decay_param[1],
        w_out[1],
        first,
    )
    second = lax.psum_scatter(terms, "tp", scatter_dimension=1, tiled=True).astype(jnp.bfloat16)
    return (
        second,
        jnp.stack([state_first, state_second]),
        jnp.stack([window_first, window_second]),
    )


def solution(mesh):
    placed = (
        P(None, ("dp", "tp")),
        P("dp"),
        P(None, "dp", "tp"),
        P(None, "dp", None, "tp"),
        P(None, "dp"),
        P(None, "dp", "tp"),
        P(None, "dp", "tp"),
        P(None, None, "tp"),
        P(None, None, "tp"),
        P(None, None, "tp"),
        P(None, "tp"),
        P(None, "tp", "dp"),
    )
    return jax.shard_map(
        body,
        mesh=mesh,
        in_specs=placed,
        out_specs=(P(None, ("dp", "tp")), P(None, "dp", "tp"), P(None, "dp", None, "tp")),
        check_vma=False,
    )
```

profile of v0, /device:TPU:0, one launch (start us, length us, event | category | flops | bytes accessed | tf_op | source)
XLA Modules:
  0.0 261.5 jit_solution(7721415944423887952)
XLA Ops:
  7.2 0.9 fusion.45
  8.1 42.0 %psum.21 = f32[128,1]{0,1:T(1,128)S(1)} all-reduce(f32[128,1]{0,1:T(1,128)S(1)} %bitcast.133), channel_id=1, replica_groups=mesh['tp'=8,'dp'=4] {'tp','dp'}, use_global_device_ids=true, to_apply=%region_1.0 | all-reduce | flops 128 | bytes 1024 | tf_op jit(solution)/shard_map/psum | solution.py:30
  50.1 1.4 fusion.76
  51.5 0.8 fusion.47
  52.3 26.4 %all_gather.9 = bf16[128,1024]{1,0:T(8,128)(2,1)S(1)} all-gather(bf16[128,128]{1,0:T(8,128)(2,1)S(1)} %fusion.47), channel_id=1, replica_groups=mesh['tp'=8,'dp'=4] {'tp'}, dimensions={1}, use_global_device_ids=true | all-gather | bytes 294912 | tf_op jit(solution)/shard_map/all_gather | solution.py:32
  78.7 1.6 convolution_convert_fusion.2
  80.4 1.5 convolution_convert_fusion.3
  81.9 0.7 pad_maximum_fusion
  82.8 1.2 fusion.74
  84.1 0.1 broadcast_compare_fusion
  84.2 0.5 broadcast_compare_fusion.1
  84.7 0.8 copy.52
  85.5 0.1 copy.51
  85.7 1.0 bitcast_select_fusion.1
  86.8 14.5 %reduce-scatter.4.cloned.1.call-done = bf16[32,1024]{1,0:T(8,128)(2,1)} async-done(((bf16[128,1024]{1,0:T(8,128)(2,1)}), bf16[32,1024]{1,0:T(8,128)(2,1)}) %reduce-scatter.4.cloned.1.call-update) | async-done | bytes 65552 | tf_op jit(solution)/shard_map/reduce_scatter | solution.py:78
  101.3 0.8 slice_bitcast_fusion.1
  102.1 1.2 fusion.8
  103.3 0.6 copy-done.12
  103.9 0.2 fusion.11
  104.2 0.9 fusion.37
  105.0 5.4 %all_gather.10 = bf16[128,512]{1,0:T(8,128)(2,1)S(1)} all-gather(bf16[32,512]{1,0:T(8,128)(2,1)S(1)} %fusion.37), channel_id=1, replica_groups=mesh['tp'=8,'dp'=4] {'dp'}, dimensions={0}, use_global_device_ids=true | all-gather | bytes 163840 | tf_op jit(solution)/shard_map/all_gather | solution.py:110
  110.4 0.3 fusion.16
  110.8 43.3 %all-reduce.1 = bf16[128,1024]{1,0:T(8,128)(2,1)S(1)} all-reduce(f32[128,1024]{1,0:T(8,128)S(1)} %fusion.48), channel_id=1, replica_groups=mesh['tp'=8,'dp'=4] {'tp'}, use_global_device_ids=true, to_apply=%region_4.5 | all-reduce | flops 131072 | bytes 786432 | tf_op jit(solution)/shard_map/psum | solution.py:150
  154.1 0.1 fusion.26
  154.2 5.9 %psum.23 = f32[128,1]{0,1:T(1,128)S(1)} all-reduce(f32[128,1]{0,1:T(1,128)S(1)} %bitcast.134), channel_id=1, replica_groups=mesh['tp'=8,'dp'=4] {'dp'}, use_global_device_ids=true, to_apply=%region_6.7 | all-reduce | flops 128 | bytes 1024 | tf_op jit(solution)/shard_map/psum | solution.py:152
  160.2 1.6 convolution_convert_fusion
  161.8 1.6 convolution_convert_fusion.1
  163.4 0.7 pad_maximum_fusion.1
  164.2 0.1 copy.54
  164.3 0.1 copy.53
  164.5 16.2 %reduce-scatter.6.cloned.1.call-done = bf16[32,1024]{1,0:T(8,128)(2,1)} async-done(((bf16[128,1024]{1,0:T(8,128)(2,1)}), bf16[32,1024]{1,0:T(8,128)(2,1)}) %reduce-scatter.6.cloned.1.call-update) | async-done | bytes 65552 | tf_op jit(solution)/shard_map/reduce_scatter | solution.py:78
  180.7 0.8 slice_bitcast_fusion
  181.5 0.2 fusion.2
  181.7 0.2 fusion.5
  182.0 0.6 copy-done.13
  182.5 0.9 fusion.42
  183.4 5.5 %all_gather.11 = bf16[128,512]{1,0:T(8,128)(2,1)S(1)} all-gather(bf16[32,512]{1,0:T(8,128)(2,1)S(1)} %fusion.42), channel_id=1, replica_groups=mesh['tp'=8,'dp'=4] {'dp'}, dimensions={0}, use_global_device_ids=true | all-gather | bytes 163840 | tf_op jit(solution)/shard_map/all_gather | solution.py:110
  189.0 0.3 fusion.12
  189.4 0.8 copy-done
  190.2 0.9 copy.34
  191.1 0.1 div.87
  191.1 0.9 copy.30
  192.1 0.9 copy.42
  193.2 0.1 fusion.39
  193.4 0.7 pad_maximum_fusion.5
  194.0 0.7 pad_maximum_fusion.2
  194.7 58.8 %reduce-scatter.8.cloned.1.call-done = f32[128,128]{1,0:T(8,128)} async-done(((f32[128,1024]{1,0:T(8,128)}), f32[128,128]{1,0:T(8,128)}) %reduce-scatter.8.cloned.1.call-update) | async-done | bytes 65552 | tf_op jit(solution)/shard_map/reduce_scatter | solution.py:170
  253.5 1.5 convert_element_type.132
  (66 shorter events, 0.7 us)
Async XLA Ops:
  7.2 94.1 %reduce-scatter.4.cloned.1.call-start = ((), (), s32[]{:S(2)}) async-start(), calls=%async_computation.3 | async-start | bytes 327680 | tf_op jit(solution)/shard_map/reduce_scatter | solution.py:78
  78.7 4.0 %copy-start.19 = (f32[2,512]{1,0:T(2,128)S(1)}, f32[2,512]{1,0:T(2,128)}, u32[]{:S(2)}) copy-start(f32[2,512]{1,0:T(2,128)} %param.22) | copy-start | bytes 12292
  78.7 4.0 %copy-start.4 = (bf16[2,256,512]{2,1,0:T(8,128)(2,1)S(1)}, bf16[2,256,512]{2,1,0:T(8,128)(2,1)}, u32[]{:S(2)}) copy-start(bf16[2,256,512]{2,1,0:T(8,128)(2,1)} %param.20) | copy-start | bytes 1572868
  80.3 3.7 %copy-start.20 = (s32[32]{0:T(128)S(1)}, s32[32]{0:T(128)}, u32[]{:S(2)}) copy-start(s32[32]{0:T(128)} %param.13) | copy-start | bytes 388
  82.6 3.0 %copy-start.16 = (bf16[2,4,512]{2,1,0:T(4,128)(2,1)S(1)}, bf16[2,4,512]{2,1,0:T(4,128)(2,1)}, u32[]{:S(2)}) copy-start(bf16[2,4,512]{2,1,0:T(4,128)(2,1)} %param.19) | copy-start | bytes 24580
  82.7 98.0 %reduce-scatter.6.cloned.1.call-start = ((), (), s32[]{:S(2)}) async-start(), calls=%async_computation.4 | async-start | bytes 327680 | tf_op jit(solution)/shard_map/reduce_scatter | solution.py:78
  82.8 21.3 %copy-start.5 = (f32[2,32,512]{2,1,0:T(8,128)S(1)}, f32[2,32,512]{2,1,0:T(8,128)}, u32[]{:S(2)}) copy-start(f32[2,32,512]{2,1,0:T(8,128)} %param.14) | copy-start | bytes 393220
  82.8 27.6 %copy-start.1 = (bf16[2,512,1024]{2,1,0:T(8,128)(2,1)S(1)}, bf16[2,512,1024]{2,1,0:T(8,128)(2,1)}, u32[]{:S(2)}) copy-start(bf16[2,512,1024]{2,1,0:T(8,128)(2,1)} %param.23) | copy-start | bytes 6291460
  85.7 25.1 %copy-start.8 = (bf16[128,128]{1,0:T(8,128)(2,1)S(1)}, bf16[128,128]{1,0:T(8,128)(2,1)}, u32[]{:S(2)}) copy-start(bf16[128,128]{1,0:T(8,128)(2,1)} %param.12) | copy-start | bytes 98308
  86.8 24.0 %copy-start.2 = (bf16[32,3,512]{2,0,1:T(8,128)(2,1)}, bf16[32,3,512]{2,0,1:T(8,128)(2,1)S(1)}, u32[]{:S(2)}) copy-start(bf16[32,3,512]{2,0,1:T(8,128)(2,1)S(1)} %get-tuple-element.8) | copy-start | bytes 294916
  102.1 2.1 copy-start.9
  103.3 0.6 copy-start.12
  104.1 0.9 copy-start.11
  163.4 19.2 %copy-start.6 = (f32[2,32,512]{2,1,0:T(8,128)S(1)}, f32[2,32,512]{2,1,0:T(8,128)}, u32[]{:S(2)}) copy-start(f32[2,32,512]{2,1,0:T(8,128)} %param.14) | copy-start | bytes 393220
  163.4 19.1 %copy-start.17 = (pred[32]{0:T(512)(128)(4,1)S(1)}, pred[32]{0:T(512)(128)(4,1)}, u32[]{:S(2)}) copy-start(pred[32]{0:T(512)(128)(4,1)} %broadcast_compare_fusion.1) | copy-start | bytes 100
  164.1 89.4 %reduce-scatter.8.cloned.1.call-start = ((), (), s32[]{:S(2)}) async-start(), calls=%async_computation.5 | async-start | bytes 589824 | tf_op jit(solution)/shard_map/reduce_scatter | solution.py:170
  181.7 1.7 copy-start.15
  181.7 10.4 %copy-start.3 = (bf16[32,3,512]{2,0,1:T(8,128)(2,1)S(1)}, bf16[32,3,512]{2,0,1:T(8,128)(2,1)}, u32[]{:S(2)}) copy-start(bf16[32,3,512]{2,0,1:T(8,128)(2,1)} %copy-done.2) | copy-start | bytes 294916
  181.9 0.6 copy-start.13
  183.4 9.7 %copy-start.14 = (f32[2,32,256]{2,1,0:T(8,128)S(1)}, f32[2,32,256]{2,1,0:T(8,128)}, u32[]{:S(2)}) copy-start(f32[2,32,256]{2,1,0:T(8,128)} %copy-done.13) | copy-start | bytes 196612
  183.4 9.8 %copy-start.7 = (f32[2,32,512]{2,1,0:T(8,128)S(1)}, f32[2,32,512]{2,1,0:T(8,128)}, u32[]{:S(2)}) copy-start(f32[2,32,512]{2,1,0:T(8,128)} %param.14) | copy-start | bytes 393220
  183.4 9.8 %copy-start.10 = (bf16[32,512]{1,0:T(8,128)(2,1)S(1)}, bf16[32,512]{1,0:T(8,128)(2,1)}, u32[]{:S(2)}) copy-start(bf16[32,512]{1,0:T(8,128)(2,1)} %copy-done.9) | copy-start | bytes 98308
  183.4 9.8 %copy-start.18 = (pred[32]{0:T(512)(128)(4,1)S(1)}, pred[32]{0:T(512)(128)(4,1)}, u32[]{:S(2)}) copy-start(pred[32]{0:T(512)(128)(4,1)} %broadcast_compare_fusion.1) | copy-start | bytes 100
  189.3 0.8 copy-start
Sparse Core Ops, SparseCore 0:
  82.8 18.4 reduce-scatter.3
  164.3 16.3 reduce-scatter.5
  190.3 63.2 reduce-scatter.7
where the time goes:
time: 263 us; the launch traced here: 262 us
  blocking collectives  129 us (49%)
  waiting for transfers between devices  89.6 us (34%)
  between operations  14.3 us (5%)
  local copies, waits for them, and re-layouts  10.4 us (4%)
  other arithmetic  9.79 us (4%)
  matrix products  8.71 us (3%)
    reduce_scatter x1, waiting for transfers between devices, body(): lax.psum_scatter(terms, 'tp', scatter_dimension=1, tiled=True)  58.8 us
    psum x1, blocking collectives, body(): carried = lax.psum(terms, 'tp').astype(jnp.bfloat16)  43.3 us
    psum x1, blocking collectives, normed_input(): lax.psum(jnp.sum(widened * widened, axis=1, keepdims=True), ('tp', 'dp'))  42 us
    reduce_scatter x2, waiting for transfers between devices, recurrent_step(): lax.psum_scatter(jnp.concatenate([jnp.dot(normed, w_branch, preferred_ele...  30.7 us
    all_gather x1, blocking collectives, normed_input(): lax.all_gather(norm_rows(stream_local, own_gain, squares), 'tp', axis=1,...  26.4 us
    all_gather x2, blocking collectives, recurrent_step(): lax.all_gather(readout, 'dp', axis=0, tiled=True)  11 us
    psum x1, blocking collectives, body(): squares = lax.psum(jnp.sum(widened * widened, axis=1, keepdims=True), 'dp')  5.93 us
  transfers between devices with their start and end apart: 3, of which 3 were waited for; matrix products, arithmetic and copies ran while one was open for 3% of the time, Pallas kernels for 0%

commit v1 on v0

--- a/solution.py
+++ b/solution.py
@@ -27,7 +27,7 @@
     own_width = stream_local.shape[1]
     offset = lax.axis_index("tp") * own_width
     widened = stream_local.astype(jnp.float32)
-    squares = lax.psum(jnp.sum(widened * widened, axis=1, keepdims=True), ("tp", "dp"))
+    squares = lax.psum(lax.psum(jnp.sum(widened * widened, axis=1, keepdims=True), "tp"), "dp")
     own_gain = lax.dynamic_slice_in_dim(gain_block, offset, own_width, 0)
     result = lax.all_gather(norm_rows(stream_local, own_gain, squares), "tp", axis=1, tiled=True)
     return result

time: 263 us -> 249 us (0.947)
  blocking collectives: 129 us -> 115 us
    psum x1 -> x2, blocking collectives: 42 us -> 28.8 us  [the longest x1 23.2 us: normed_input(): lax.psum(jnp.sum(widened * widened, axis=1, keepdims=True), 'tp')]
where the time goes in v1:
time: 249 us; the launch traced here: 247 us
  blocking collectives  115 us (46%)
  waiting for transfers between devices  88.7 us (36%)
  between operations  14.3 us (6%)
  local copies, waits for them, and re-layouts  10.5 us (4%)
  other arithmetic  9.79 us (4%)
  matrix products  8.69 us (3%)
    reduce_scatter x1, waiting for transfers between devices, body(): lax.psum_scatter(terms, 'tp', scatter_dimension=1, tiled=True)  58.8 us
    psum x1, blocking collectives, body(): carried = lax.psum(terms, 'tp').astype(jnp.bfloat16)  43.3 us
    reduce_scatter x2, waiting for transfers between devices, recurrent_step(): lax.psum_scatter(jnp.concatenate([jnp.dot(normed, w_branch, preferred_ele...  29.8 us
    all_gather x1, blocking collectives, normed_input(): lax.all_gather(norm_rows(stream_local, own_gain, squares), 'tp', axis=1,...  26.4 us
    psum x1, blocking collectives, normed_input(): lax.psum(jnp.sum(widened * widened, axis=1, keepdims=True), 'tp')  23.2 us
    all_gather x2, blocking collectives, recurrent_step(): lax.all_gather(readout, 'dp', axis=0, tiled=True)  11 us
    psum x1, blocking collectives, body(): squares = lax.psum(jnp.sum(widened * widened, axis=1, keepdims=True), 'dp')  5.93 us
    psum x1, blocking collectives, normed_input(): lax.psum(lax.psum(jnp.sum(widened * widened, axis=1, keepdims=True), 'tp'...  5.65 us
  transfers between devices with their start and end apart: 3, of which 3 were waited for; matrix products, arithmetic and copies ran while one was open for 3% of the time, Pallas kernels for 0%

profile of v1, /device:TPU:0, one launch (start us, length us, event | category | flops | bytes accessed | tf_op | source)
XLA Modules:
  0.0 247.5 jit_solution(14357538530264192292)
XLA Ops:
  7.2 0.9 fusion.45
  8.1 23.2 %psum.28 = f32[128,1]{0,1:T(1,128)S(1)} all-reduce(f32[128,1]{0,1:T(1,128)S(1)} %bitcast.133), channel_id=1, replica_groups=mesh['tp'=8,'dp'=4] {'tp'}, use_global_device_ids=true, to_apply=%region_1.0 | all-reduce | flops 128 | bytes 1024 | tf_op jit(solution)/shard_map/psum | solution.py:30
  31.2 5.6 %psum.29 = f32[128,1]{0,1:T(1,128)S(1)} all-reduce(f32[128,1]{0,1:T(1,128)S(1)} %psum.28), channel_id=1, replica_groups=mesh['tp'=8,'dp'=4] {'dp'}, use_global_device_ids=true, to_apply=%region_2.0 | all-reduce | flops 128 | bytes 1024 | tf_op jit(solution)/shard_map/psum | solution.py:30
  36.9 1.4 fusion.76
  38.3 0.8 fusion.47
  39.1 26.4 %all_gather.9 = bf16[128,1024]{1,0:T(8,128)(2,1)S(1)} all-gather(bf16[128,128]{1,0:T(8,128)(2,1)S(1)} %fusion.47), channel_id=1, replica_groups=mesh['tp'=8,'dp'=4] {'tp'}, dimensions={1}, use_global_device_ids=true | all-gather | bytes 294912 | tf_op jit(solution)/shard_map/all_gather | solution.py:32
  65.6 1.6 convolution_convert_fusion.2
  67.2 1.5 convolution_convert_fusion.3
  68.7 0.7 pad_maximum_fusion
  69.7 1.2 fusion.74
  70.9 0.1 broadcast_compare_fusion
  71.0 0.6 broadcast_compare_fusion.1
  71.5 0.8 copy.52
  72.4 0.1 copy.51
  72.5 1.0 bitcast_select_fusion.1
  73.6 13.6 %reduce-scatter.4.cloned.1.call-done = bf16[32,1024]{1,0:T(8,128)(2,1)} async-done(((bf16[128,1024]{1,0:T(8,128)(2,1)}), bf16[32,1024]{1,0:T(8,128)(2,1)}) %reduce-scatter.4.cloned.1.call-update) | async-done | bytes 65552 | tf_op jit(solution)/shard_map/reduce_scatter | solution.py:78
  87.2 0.8 slice_bitcast_fusion.1
  88.0 1.2 fusion.8
  89.2 0.6 copy-done.12
  89.8 0.2 fusion.11
  90.0 0.9 fusion.37
  90.9 5.4 %all_gather.10 = bf16[128,512]{1,0:T(8,128)(2,1)S(1)} all-gather(bf16[32,512]{1,0:T(8,128)(2,1)S(1)} %fusion.37), channel_id=1, replica_groups=mesh['tp'=8,'dp'=4] {'dp'}, dimensions={0}, use_global_device_ids=true | all-gather | bytes 163840 | tf_op jit(solution)/shard_map/all_gather | solution.py:110
  96.3 0.3 fusion.16
  96.7 43.3 %all-reduce.1 = bf16[128,1024]{1,0:T(8,128)(2,1)S(1)} all-reduce(f32[128,1024]{1,0:T(8,128)S(1)} %fusion.48), channel_id=1, replica_groups=mesh['tp'=8,'dp'=4] {'tp'}, use_global_device_ids=true, to_apply=%region_5.6 | all-reduce | flops 131072 | bytes 786432 | tf_op jit(solution)/shard_map/psum | solution.py:150
  140.0 0.1 fusion.26
  140.1 5.9 %psum.31 = f32[128,1]{0,1:T(1,128)S(1)} all-reduce(f32[128,1]{0,1:T(1,128)S(1)} %bitcast.134), channel_id=1, replica_groups=mesh['tp'=8,'dp'=4] {'dp'}, use_global_device_ids=true, to_apply=%region_7.8 | all-reduce | flops 128 | bytes 1024 | tf_op jit(solution)/shard_map/psum | solution.py:152
  146.1 1.6 convolution_convert_fusion
  147.7 1.6 convolution_convert_fusion.1
  149.3 0.7 pad_maximum_fusion.1
  150.1 0.1 copy.54
  150.2 0.1 copy.53
  150.4 16.2 %reduce-scatter.6.cloned.1.call-done = bf16[32,1024]{1,0:T(8,128)(2,1)} async-done(((bf16[128,1024]{1,0:T(8,128)(2,1)}), bf16[32,1024]{1,0:T(8,128)(2,1)}) %reduce-scatter.6.cloned.1.call-update) | async-done | bytes 65552 | tf_op jit(solution)/shard_map/reduce_scatter | solution.py:78
  166.6 0.8 slice_bitcast_fusion
  167.3 0.2 fusion.2
  167.6 0.2 fusion.5
  167.8 0.6 copy-done.13
  168.4 0.9 fusion.42
  169.3 5.5 %all_gather.11 = bf16[128,512]{1,0:T(8,128)(2,1)S(1)} all-gather(bf16[32,512]{1,0:T(8,128)(2,1)S(1)} %fusion.42), channel_id=1, replica_groups=mesh['tp'=8,'dp'=4] {'dp'}, dimensions={0}, use_global_device_ids=true | all-gather | bytes 163840 | tf_op jit(solution)/shard_map/all_gather | solution.py:110
  174.9 0.3 fusion.12
  175.2 0.8 copy-done
  176.1 0.9 copy.34
  177.0 0.9 copy.30
  178.0 0.9 copy.42
  179.1 0.1 fusion.39
  179.3 0.7 pad_maximum_fusion.5
  179.9 0.7 pad_maximum_fusion.2
  180.6 58.8 %reduce-scatter.8.cloned.1.call-done = f32[128,128]{1,0:T(8,128)} async-done(((f32[128,1024]{1,0:T(8,128)}), f32[128,128]{1,0:T(8,128)}) %reduce-scatter.8.cloned.1.call-update) | async-done | bytes 65552 | tf_op jit(solution)/shard_map/reduce_scatter | solution.py:170
  239.5 1.5 convert_element_type.132
  (67 shorter events, 0.8 us)
Async XLA Ops:
  7.2 80.0 %reduce-scatter.4.cloned.1.call-start = ((), (), s32[]{:S(2)}) async-start(), calls=%async_computation.3 | async-start | bytes 327680 | tf_op jit(solution)/shard_map/reduce_scatter | solution.py:78
  65.6 4.0 %copy-start.19 = (f32[2,512]{1,0:T(2,128)S(1)}, f32[2,512]{1,0:T(2,128)}, u32[]{:S(2)}) copy-start(f32[2,512]{1,0:T(2,128)} %param.22) | copy-start | bytes 12292
  65.6 4.0 %copy-start.4 = (bf16[2,256,512]{2,1,0:T(8,128)(2,1)S(1)}, bf16[2,256,512]{2,1,0:T(8,128)(2,1)}, u32[]{:S(2)}) copy-start(bf16[2,256,512]{2,1,0:T(8,128)(2,1)} %param.20) | copy-start | bytes 1572868
  67.2 3.7 %copy-start.20 = (s32[32]{0:T(128)S(1)}, s32[32]{0:T(128)}, u32[]{:S(2)}) copy-start(s32[32]{0:T(128)} %param.13) | copy-start | bytes 388
  69.4 3.1 %copy-start.16 = (bf16[2,4,512]{2,1,0:T(4,128)(2,1)S(1)}, bf16[2,4,512]{2,1,0:T(4,128)(2,1)}, u32[]{:S(2)}) copy-start(bf16[2,4,512]{2,1,0:T(4,128)(2,1)} %param.19) | copy-start | bytes 24580
  69.5 97.1 %reduce-scatter.6.cloned.1.call-start = ((), (), s32[]{:S(2)}) async-start(), calls=%async_computation.4 | async-start | bytes 327680 | tf_op jit(solution)/shard_map/reduce_scatter | solution.py:78
  69.6 20.4 %copy-start.5 = (f32[2,32,512]{2,1,0:T(8,128)S(1)}, f32[2,32,512]{2,1,0:T(8,128)}, u32[]{:S(2)}) copy-start(f32[2,32,512]{2,1,0:T(8,128)} %param.14) | copy-start | bytes 393220
  69.6 26.7 %copy-start.1 = (bf16[2,512,1024]{2,1,0:T(8,128)(2,1)S(1)}, bf16[2,512,1024]{2,1,0:T(8,128)(2,1)}, u32[]{:S(2)}) copy-start(bf16[2,512,1024]{2,1,0:T(8,128)(2,1)} %param.23) | copy-start | bytes 6291460
  72.5 24.1 %copy-start.8 = (bf16[128,128]{1,0:T(8,128)(2,1)S(1)}, bf16[128,128]{1,0:T(8,128)(2,1)}, u32[]{:S(2)}) copy-start(bf16[128,128]{1,0:T(8,128)(2,1)} %param.12) | copy-start | bytes 98308
  73.6 23.1 %copy-start.2 = (bf16[32,3,512]{2,0,1:T(8,128)(2,1)}, bf16[32,3,512]{2,0,1:T(8,128)(2,1)S(1)}, u32[]{:S(2)}) copy-start(bf16[32,3,512]{2,0,1:T(8,128)(2,1)S(1)} %get-tuple-element.8) | copy-start | bytes 294916
  88.0 2.1 copy-start.9
  89.2 0.6 copy-start.12
  90.0 0.9 copy-start.11
  149.3 19.2 %copy-start.6 = (f32[2,32,512]{2,1,0:T(8,128)S(1)}, f32[2,32,512]{2,1,0:T(8,128)}, u32[]{:S(2)}) copy-start(f32[2,32,512]{2,1,0:T(8,128)} %param.14) | copy-start | bytes 393220
  149.3 19.2 %copy-start.17 = (pred[32]{0:T(512)(128)(4,1)S(1)}, pred[32]{0:T(512)(128)(4,1)}, u32[]{:S(2)}) copy-start(pred[32]{0:T(512)(128)(4,1)} %broadcast_compare_fusion.1) | copy-start | bytes 100
  150.0 89.4 %reduce-scatter.8.cloned.1.call-start = ((), (), s32[]{:S(2)}) async-start(), calls=%async_computation.5 | async-start | bytes 589824 | tf_op jit(solution)/shard_map/reduce_scatter | solution.py:170
  167.6 1.7 copy-start.15
  167.6 10.4 %copy-start.3 = (bf16[32,3,512]{2,0,1:T(8,128)(2,1)S(1)}, bf16[32,3,512]{2,0,1:T(8,128)(2,1)}, u32[]{:S(2)}) copy-start(bf16[32,3,512]{2,0,1:T(8,128)(2,1)} %copy-done.2) | copy-start | bytes 294916
  167.8 0.6 copy-start.13
  169.3 9.7 %copy-start.14 = (f32[2,32,256]{2,1,0:T(8,128)S(1)}, f32[2,32,256]{2,1,0:T(8,128)}, u32[]{:S(2)}) copy-start(f32[2,32,256]{2,1,0:T(8,128)} %copy-done.13) | copy-start | bytes 196612
  169.3 9.8 %copy-start.7 = (f32[2,32,512]{2,1,0:T(8,128)S(1)}, f32[2,32,512]{2,1,0:T(8,128)}, u32[]{:S(2)}) copy-start(f32[2,32,512]{2,1,0:T(8,128)} %param.14) | copy-start | bytes 393220
  169.3 9.8 %copy-start.10 = (bf16[32,512]{1,0:T(8,128)(2,1)S(1)}, bf16[32,512]{1,0:T(8,128)(2,1)}, u32[]{:S(2)}) copy-start(bf16[32,512]{1,0:T(8,128)(2,1)} %copy-done.9) | copy-start | bytes 98308
  169.3 9.8 %copy-start.18 = (pred[32]{0:T(512)(128)(4,1)S(1)}, pred[32]{0:T(512)(128)(4,1)}, u32[]{:S(2)}) copy-start(pred[32]{0:T(512)(128)(4,1)} %broadcast_compare_fusion.1) | copy-start | bytes 100
  175.2 0.8 copy-start
Sparse Core Ops, SparseCore 0:
  69.6 17.5 reduce-scatter.3
  150.2 16.3 reduce-scatter.5
  176.2 63.2 reduce-scatter.7
